TPU v7x, 32 devices: a whole 2x2x4 slice. The times are simulated.
32 devices in a mesh: sp: 8 (over z, x), tp: 4 (over y, core).
Axes of the slice: x: 2, y: 2, z: 4, core: 2. Of those that a mesh axis runs over, the one named last changes fastest.
Arguments:
- inputs: bfloat16 [3072, 2048], P('sp', 'tp'), may hold values from -6 to 6
- norm_gain: float32 [2048], replicated, may hold values from 0.1 to 1.9
- query_weight: bfloat16 [2048, 1024], P(None, 'tp')
- key_weight: bfloat16 [2048, 1024], P(None, 'tp'), may hold values from -0.15625 to 0.15625
- value_weight: bfloat16 [2048, 1024], P(None, 'tp'), may hold values from -0.125 to 0.125
- memory_query_weight: bfloat16 [2048, 1024], P(None, 'tp'), may hold values from -0.125 to 0.125
- memory_key_weight: bfloat16 [2048, 1024], P(None, 'tp'), may hold values from -0.125 to 0.125
- memory_value_weight: bfloat16 [2048, 1024], P(None, 'tp'), may hold values from -0.125 to 0.125
- input_gate_weight: bfloat16 [2048, 16], P(None, 'tp')
- forget_gate_weight: bfloat16 [2048, 16], P(None, 'tp'), may hold values from -0.3125 to 0.3125
- forget_bias: float32 [16], P('tp'), may hold values from 3 to 13
- decay_shift: float32 [3072, 16], P('sp', 'tp'), may hold values from -2 to 0, as said below
- lambdas: float32 [16], P('tp'), may hold values from 0.3 to 0.8
- head_gain: float32 [64], replicated, may hold values from 0.1 to 1.9
- out_weight_attention: bfloat16 [1024, 2048], P('tp'), may hold values from -0.125 to 0.125
- out_weight_memory: bfloat16 [1024, 2048], P('tp'), may hold values from -0.125 to 0.125
Outputs:
- combined: bfloat16 [3072, 2048], P('sp', 'tp')
Inputs may be any that keep to these rules, and one draw needn't show every extreme that they name: `decay_shift`: never positive.
All inputs are finite; a program needn't handle non-finite values.
Results may differ from a plain program's by a relative error of at most 0.018.
The roundings to bfloat16 on the way count: a program that leaves them out, or rounds other values in their place, can miss the bound.
Values may be sent and summed in bfloat16 or wider, within the bound.
A program may use at most 192 MiB of HBM per device.

v0:
```python
import jax
import jax.numpy as jnp
from jax import lax
from jax.sharding import PartitionSpec as P

HEAD = 64
DD = 32
BLOCK = 64
EPSILON = 1e-06
ROTARY_BASE = 10000.0
NEGATIVE = -1e30


def carried_in(part, axis, combine, identity):
    place = lax.axis_index(axis)
    gathered = jax.tree.map(lambda a: lax.all_gather(a, axis), part)
    state = jax.tree.map(lambda a, e: jnp.zeros_like(a) + jnp.asarray(e, a.dtype), part, identity)

    def one(hop, state):
        return combine(
            state, jax.tree.map(lambda a: lax.dynamic_index_in_dim(a, hop, 0, False), gathered)
        )

    return lax.fori_loop(0, place, one, state)


def rotate(halves, positions):
    middle = halves.shape[-1] // 2
    inverse = 1.0 / ROTARY_BASE ** (jnp.arange(middle, dtype=jnp.float32) / middle)
    angles = positions.astype(jnp.float32)[:, None] * inverse[None, :]
    cosine = jnp.cos(angles)[:, None, :]
    sine_part = jnp.sin(angles)[:, None, :]
    floats = halves.astype(jnp.float32)
    former = floats[..., :middle]
    latter = floats[..., middle:]
    turned = jnp.concatenate(
        [former * cosine - latter * sine_part, latter * cosine + former * sine_part], axis=-1
    )
    return turned.astype(jnp.bfloat16)


def advance_state(carried, block_entry):
    memory, normal, stable = carried
    block_memory, block_normal, block_max, block_decay = block_entry
    new_stable = jnp.maximum(block_decay + stable, block_max)
    former = jnp.exp(block_decay + stable - new_stable)
    latter = jnp.exp(block_max - new_stable)
    return (
        former[:, None, None] * memory + latter[:, None, None] * block_memory,
        former[:, None] * normal + latter[:, None] * block_normal,
        new_stable,
    )


def memory_blocks(queries, key_heads, values, gate_in, log_forget, entering):
    token_count, head_count, head_width = queries.shape
    block_count = token_count // BLOCK
    highest = lax.Precision.HIGHEST

    def blocked(flat_array):
        return (
            flat_array.astype(jnp.float32)
            .reshape(block_count, BLOCK, head_count, head_width)
            .transpose(2, 0, 1, 3)
        )

    query_blocks = blocked(queries)
    key_blocks = blocked(key_heads) * head_width ** (-0.5)
    value_blocks = blocked(values)
    gate_blocks = gate_in.reshape(block_count, BLOCK, head_count).transpose(2, 0, 1)
    cumulative = jnp.cumsum(
        log_forget.reshape(block_count, BLOCK, head_count).transpose(2, 0, 1), axis=-1
    )
    block_ends = cumulative[..., -1]
    toward_end = block_ends[..., None] - cumulative + gate_blocks
    local_max = jnp.max(toward_end, axis=-1)
    end_weights = jnp.exp(toward_end - local_max[..., None])
    local_memory = jnp.einsum(
        "hcl,hclv,hclk->chvk", end_weights, value_blocks, key_blocks, precision=highest
    )
    local_normal = jnp.einsum("hcl,hclk->chk", end_weights, key_blocks, precision=highest)

    def scan_step(carried, block_entry):
        return (advance_state(carried, block_entry), carried)

    entries = (local_memory, local_normal, local_max.T, block_ends.T)
    unused, (memory_in, normal_in, stable_in) = lax.scan(scan_step, entering, entries)
    lower_mask = jnp.tril(jnp.ones((BLOCK, BLOCK), dtype=bool))
    decays = jnp.where(
        lower_mask,
        cumulative[..., :, None] - cumulative[..., None, :] + gate_blocks[..., None, :],
        NEGATIVE,
    )
    carried_log = cumulative + stable_in.T[..., None]
    row_max = jnp.maximum(carried_log, jnp.max(decays, axis=-1))
    within = jnp.where(lower_mask, jnp.exp(decays - row_max[..., None]), 0.0)
    outside = jnp.exp(carried_log - row_max)
    scores = within * jnp.einsum("hctd,hcsd->hcts", query_blocks, key_blocks, precision=highest)
    numerator = outside[..., None] * jnp.einsum(
        "chvk,hctk->hctv", memory_in, query_blocks, precision=highest
    )
    numerator = numerator + jnp.einsum("hcts,hcsv->hctv", scores, value_blocks, precision=highest)
    denominator = outside * jnp.einsum(
        "chk,hctk->hct", normal_in, query_blocks, precision=highest
    ) + jnp.sum(scores, axis=-1)
    result = numerator / jnp.maximum(jnp.abs(denominator), 1.0)[..., None]
    return (
        result.transpose(1, 2, 0, 3)
        .reshape(token_count, head_count * head_width)
        .astype(jnp.bfloat16)
    )


def combine_states(earlier, later_part):
    memory, normal, stable, decay_sum = earlier
    later_memory, later_normal, later_stable, later_decay = later_part
    new_stable = jnp.maximum(later_decay + stable, later_stable)
    former = jnp.exp(later_decay + stable - new_stable)
    latter = jnp.exp(later_stable - new_stable)
    return (
        former[:, None, None] * memory + latter[:, None, None] * later_memory,
        former[:, None] * normal + latter[:, None] * later_normal,
        new_stable,
        decay_sum + later_decay,
    )


def summarize(key_heads, values, gate_in, log_forget):
    head_width = key_heads.shape[-1]
    highest = lax.Precision.HIGHEST
    key_floats = key_heads.astype(jnp.float32) * head_width ** (-0.5)
    cumulative = jnp.cumsum(log_forget, axis=0)
    span_decay = cumulative[-1]
    toward_end = span_decay[None, :] - cumulative + gate_in
    span_max = jnp.max(toward_end, axis=0)
    end_weights = jnp.exp(toward_end - span_max[None, :])
    memory = jnp.einsum(
        "rh,rhv,rhk->hvk", end_weights, values.astype(jnp.float32), key_floats, precision=highest
    )
    normal = jnp.einsum("rh,rhk->hk", end_weights, key_floats, precision=highest)
    return (memory, normal, span_max, span_decay)


def attend(carried, arriving, query_first, query_second, query_positions):
    key_first = arriving[..., :DD]
    key_second = arriving[..., DD : 2 * DD]
    value_part = arriving[..., 2 * DD :]
    key_positions = jnp.arange(arriving.shape[0], dtype=jnp.int32)
    visible = (key_positions[None, :] <= query_positions[:, None]) & (key_positions[None, :] >= 0)
    score_scale = DD ** (-0.5)
    results = []
    for side_index, (query_side, key_side) in enumerate(
        ((query_first, key_first), (query_second, key_second))
    ):
        row_max, totals, accumulated = carried[3 * side_index : 3 * side_index + 3]
        scores = (
            jnp.einsum("qhd,khd->hqk", query_side, key_side, preferred_element_type=jnp.float32)
            * score_scale
        )
        scores = jnp.where(visible[None], scores, NEGATIVE)
        new_max = jnp.maximum(row_max, jnp.max(scores, axis=2))
        weights = jnp.where(visible[None], jnp.exp(scores - new_max[..., None]), 0.0)
        totals = jnp.sum(weights, axis=2)
        accumulated = jnp.einsum(
            "hqk,khd->hqd",
            weights.astype(jnp.bfloat16),
            value_part,
            preferred_element_type=jnp.float32,
        )
        results.extend([new_max, totals, accumulated])
    return tuple(results)


def per_device(
    inputs,
    norm_gain,
    query_weight,
    key_weight,
    value_weight,
    memory_query_weight,
    memory_key_weight,
    memory_value_weight,
    input_gate_weight,
    forget_gate_weight,
    forget_bias,
    decay_shift,
    lambdas,
    head_gain,
    out_weight_attention,
    out_weight_memory,
):
    row_count = inputs.shape[0]
    weights = (
        query_weight,
        key_weight,
        value_weight,
        memory_query_weight,
        memory_key_weight,
        memory_value_weight,
        input_gate_weight,
        forget_gate_weight,
    )
    floats = lax.all_gather(inputs, "tp", axis=1, tiled=True).astype(jnp.float32)
    scaled = (floats * norm_gain[None, :]).astype(jnp.bfloat16)
    running_sums = tuple(
        (jnp.dot(scaled, weight, preferred_element_type=jnp.float32) for weight in weights)
    )
    running_sums, squares = (running_sums, jnp.sum(floats * floats, axis=1))
    inverse_rms = lax.rsqrt(squares / norm_gain.shape[0] + EPSILON)[:, None]
    projected = [running * inverse_rms for running in running_sums]

    def split_heads(flat_values):
        return flat_values.astype(jnp.bfloat16).reshape(row_count, -1, HEAD)

    queries = split_heads(projected[0])
    key_heads = split_heads(projected[1])
    values = split_heads(projected[2])
    offset = lax.axis_index("sp") * row_count
    positions = offset + jnp.arange(row_count, dtype=jnp.int32)
    query_first = rotate(queries[..., :DD], positions)
    query_second = rotate(queries[..., DD:], positions)
    packed = jnp.concatenate(
        [rotate(key_heads[..., :DD], positions), rotate(key_heads[..., DD:], positions), values],
        axis=-1,
    )
    head_count = queries.shape[1]
    empty_max = jnp.full((head_count, row_count), NEGATIVE, jnp.float32)
    empty_total = jnp.zeros((head_count, row_count), jnp.float32)
    empty_sums = jnp.zeros((head_count, row_count, HEAD), jnp.float32)
    starting = (empty_max, empty_total, empty_sums, empty_max, empty_total, empty_sums)
    gathered = attend(
        starting,
        lax.all_gather(packed, "sp", axis=0, tiled=True),
        query_first,
        query_second,
        positions,
    )
    first_max, first_total, first_sums, second_max, second_total, second_sums = gathered
    stacked = first_sums / first_total[..., None] - lambdas[:, None, None] * (
        second_sums / second_total[..., None]
    )
    stacked = stacked.transpose(1, 0, 2)
    norm_scale = lax.rsqrt(jnp.mean(stacked * stacked, axis=-1, keepdims=True) + EPSILON)
    attended = (stacked * norm_scale * head_gain).astype(jnp.bfloat16).reshape(row_count, -1)
    gate_in = projected[6]
    log_forget = jax.nn.log_sigmoid(projected[7] + forget_bias[None, :]) + decay_shift
    memory_queries = split_heads(projected[3])
    memory_keys = split_heads(projected[4])
    memory_values = split_heads(projected[5])
    summary = summarize(memory_keys, memory_values, gate_in, log_forget)
    memory_heads = gate_in.shape[1]
    identity = (
        jnp.zeros((memory_heads, HEAD, HEAD), jnp.float32),
        jnp.zeros((memory_heads, HEAD), jnp.float32),
        jnp.full((memory_heads,), NEGATIVE, jnp.float32),
        jnp.zeros((memory_heads,), jnp.float32),
    )
    prefix = carried_in(summary, "sp", combine_states, identity)
    start_state = (
        jnp.zeros((memory_heads, HEAD, HEAD), jnp.float32),
        jnp.zeros((memory_heads, HEAD), jnp.float32),
        jnp.zeros((memory_heads,), jnp.float32),
        jnp.zeros((memory_heads,), jnp.float32),
    )
    entering = combine_states(start_state, prefix)[:3]
    memory = memory_blocks(
        memory_queries, memory_keys, memory_values, gate_in, log_forget, entering
    )
    partial_term = jnp.dot(attended, out_weight_attention, preferred_element_type=jnp.float32)
    partial_term = partial_term + jnp.dot(
        memory, out_weight_memory, preferred_element_type=jnp.float32
    )
    return lax.psum_scatter(
        partial_term.astype(jnp.bfloat16), "tp", scatter_dimension=1, tiled=True
    )


def solution(mesh):
    in_specs = (
        P("sp", "tp"),
        P(),
        P(None, "tp"),
        P(None, "tp"),
        P(None, "tp"),
        P(None, "tp"),
        P(None, "tp"),
        P(None, "tp"),
        P(None, "tp"),
        P(None, "tp"),
        P("tp"),
        P("sp", "tp"),
        P("tp"),
        P(),
        P("tp", None),
        P("tp", None),
    )
    out_specs = P("sp", "tp")
    return jax.shard_map(
        per_device, mesh=mesh, in_specs=in_specs, out_specs=out_specs, check_vma=False
    )
```

profile of v0, /device:TPU:0, one launch (start us, length us, event | category | flops | bytes accessed | tf_op | source)
XLA Modules:
  0.0 310.0 jit_solution(3127829194106254127)
XLA Ops:
  6.6 0.7 all-gather.8.cloned.1.call-update
  7.4 1.2 dynamic-slice
  9.5 0.7 iota_compare_fusion
  10.2 21.1 %all-gather.8.cloned.1.call-done = bf16[384,2048]{1,0:T(8,128)(2,1)} async-done(((bf16[384,512]{1,0:T(8,128)(2,1)}), bf16[384,2048]{1,0:T(8,128)(2,1)}) %all-gather.8.cloned.1.call-update) | async-done | bytes 1572880 | tf_op jit(solution)/shard_map/all_gather | solution.py:203
  31.3 1.8 fusion.26
  33.2 1.9 fusion.113
  35.2 1.2 reduce-window.6
  37.0 2.0 fusion.128
  39.5 21.3 %all-reduce = f32[32]{0:T(128)S(1)} all-reduce(f32[32]{0:T(128)S(1)} %dynamic-update-slice), channel_id=2, replica_groups=mesh['sp'=8,'tp'=4] {'sp'}, use_global_device_ids=true, to_apply=%add | all-reduce | flops 32 | bytes 256
  60.9 16.7 %all-gather.3 = f32[8,1,4]{2,1,0:T(1,128)} all-gather(f32[1,1,4]{2,1,0:T(1,128)S(1)} %bitcast.225), channel_id=1, replica_groups=mesh['sp'=8,'tp'=4] {'sp'}, dimensions={0}, use_global_device_ids=true | all-gather | bytes 144 | tf_op jit(solution)/shard_map/all_gather | solution.py:16
  77.6 0.9 reduce_window_sum.28
  79.0 0.7 copy.60
  79.6 2.5 fusion.46
  82.5 0.8 copy.55
  83.3 2.5 fusion.49
  85.8 0.9 copy.57
  86.7 1.2 fusion.84
  88.5 26.1 %all-gather.4 = f32[8,4,64]{2,1,0:T(4,128)S(1)} all-gather(f32[1,4,64]{2,1,0:T(4,128)S(1)} %bitcast.221), channel_id=4, replica_groups=mesh['sp'=8,'tp'=4] {'sp'}, dimensions={0}, use_global_device_ids=true | all-gather | bytes 9216 | tf_op jit(solution)/shard_map/all_gather | solution.py:16
  114.6 2.5 fusion.44
  117.2 0.8 fusion.45
  118.1 0.7 copy-done.8
  118.9 1.3 mul.423
  120.2 0.8 fusion.81
  121.0 1.4 convert_multiply_fusion.2
  122.4 2.3 fusion.78
  124.7 36.9 %all-gather.1 = f32[32,64,64]{2,1,0:T(8,128)} all-gather(f32[4,64,64]{2,1,0:T(8,128)S(1)} %copy-done.7), channel_id=3, replica_groups=mesh['sp'=8,'tp'=4] {'sp'}, dimensions={0}, use_global_device_ids=true | all-gather | bytes 589824 | tf_op jit(solution)/shard_map/all_gather | solution.py:16
  162.0 18.5 %while.37 = (s32[]{:T(128)}, f32[4,64,64]{2,1,0:T(8,128)S(1)}, f32[4,64]{1,0:T(4,128)S(1)}, f32[4]{0:T(128)S(1)}, f32[6,4,64,64]{3,2,0,1:T(8,128)}, /*index=5*/f...) while((s32[]{:T(128)}, f32[4,64,64]{2,1,0:T(8,128)S(1)}, ...), condition=%wide.region_14.15_spmd, body=%wide.region_13.14_spmd.sunk | while | flops 49938 | bytes 399745 | solution.py:87
  162.0 0.7 subtract_exponential_fusion.13
  162.8 0.6 bitcast_dynamic-update-slice_fusion.5
  163.4 0.7 bitcast_dynamic-update-slice_fusion.4
  164.1 1.0 fusion.159
  165.1 0.7 subtract_exponential_fusion.13
  166.5 0.7 bitcast_dynamic-update-slice_fusion.4
  167.2 1.0 fusion.159
  168.2 0.7 subtract_exponential_fusion.13
  168.9 0.6 bitcast_dynamic-update-slice_fusion.5
  169.6 0.7 bitcast_dynamic-update-slice_fusion.4
  170.3 1.0 fusion.159
  171.3 0.7 subtract_exponential_fusion.13
  172.7 0.7 bitcast_dynamic-update-slice_fusion.4
  173.3 1.0 fusion.159
  174.4 0.7 subtract_exponential_fusion.13
  175.7 0.7 bitcast_dynamic-update-slice_fusion.4
  176.4 1.0 fusion.159
  177.4 0.7 subtract_exponential_fusion.13
  178.8 0.7 bitcast_dynamic-update-slice_fusion.4
  179.5 1.0 fusion.159
  180.5 3.1 %fusion.50 = bf16[384,256]{0,1:T(8,128)(2,1)} fusion(bf16[2048,256]{1,0:T(8,128)(2,1)} %param.25, bf16[384,2048]{1,0:T(8,128)(2,1)} %all-gather.8.cloned.1.call-done, f32[2048]{0:T(1024)S(1)} %copy-done.22, f32[384]{0:T(512)S(1)} %copy-done.11), kind=kOutput, calls=%fused_computation.71 | convolution fusion | flops 405209088 | bytes 2827776 | tf_op jit(solution)/shard_map/dot_general | solution.py:206
  183.6 1.8 copy.64
  185.4 1.9 reshape.199
  187.3 1.9 copy.80
  190.1 1.4 fusion.109
  191.5 1.7 fusion.132
  193.3 0.8 convolution_bitcast_fusion
  194.2 0.9 fusion.32
  195.7 2.5 fusion.43
  198.3 10.2 %fusion.75 = f32[4,384,3072]{2,1,0:T(8,128)} fusion(bf16[3072,4,128]{0,2,1:T(8,128)(2,1)} %all-gather.10.cloned.1.call-done, bf16[384,4,16]{0,2,1:T(8,128)(2,1)S(1)} %get-tuple-element.253, bf16[384,4,16]{0,2,1:T(8,128)(2,1)S(1)} %get-tuple-element.254), kind=kOutput, calls=%fused_computation.82 | convolution fusion | flops 302186496 | bytes 19759104 | tf_op jit(solution)/shard_map/qhd,khd->hqk/dot_general | solution.py:157
  208.5 17.6 %fusion.14 = (f32[4,384]{1,0:T(4,128)S(1)}, f32[4,384]{1,0:T(4,128)S(1)}, f32[4,384,3072]{2,1,0:T(8,128)}) fusion(pred[384,3072]{1,0:T(8,128)(4,1)S(1)} %iota_compare_fusion, f32[4,384,3072]{2,1,0:T(8,128)} %fusion.75, bf16[3072,4,128]{0,2,1:T(8,128)(2,1)} %all-gather.10.cloned.1.call-done, bf16[384,4,16]{0,2,1:T(8,128)(2,1)S(1)} %get-tuple-element.246, ...), kind=kOutput, calls=%fused_computation.32 | convolution fusion | flops 330494976 | bytes 39825408 | tf_op jit(solution)/shard_map/qhd,khd->hqk/dot_general | solution.py:157
  226.1 17.6 %fusion.17 = (f32[4,384]{1,0:T(4,128)S(1)}, f32[4,384]{1,0:T(4,128)S(1)}) fusion(f32[4,384,3072]{2,1,0:T(8,128)} %get-tuple-element.257, f32[4,384]{1,0:T(4,128)S(1)} %get-tuple-element.264, pred[384,3072]{1,0:T(8,128)(4,1)} %copy-done.2, f32[4,384]{1,0:T(4,128)S(1)} %get-tuple-element.265, f32[4,384,3072]{2,1,0:T(8,128)} %fusion.75), kind=kLoop, calls=%fused_computation.35 | loop fusion | flops 47182848 | bytes 38952960 | tf_op jit(solution)/shard_map/reduce_sum | solution.py:163
  244.0 8.0 %fusion.68 = f32[384,4,64]{0,2,1:T(8,128)S(1)} fusion(bf16[3072,4,128]{0,2,1:T(8,128)(2,1)} %all-gather.10.cloned.1.call-done, f32[4,384,3072]{2,1,0:T(8,128)S(1)} %copy-done.1, f32[4,384]{1,0:T(4,128)S(1)} %get-tuple-element.265, pred[384,3072]{1,0:T(8,128)(4,1)} %copy-done.2, f32[384,4]{0,1:T(4,128)S(1)} %bitcast.224), kind=kOutput, calls=%fused_computation.79 | convolution fusion | flops 627671040 | bytes 22032384 | tf_op jit(solution)/shard_map/hqk,khd->hqd/dot_general | solution.py:164
  252.0 9.9 %multiply_reduce_fusion = (f32[384,4]{0,1:T(4,128)S(1)}, f32[384,4,64]{0,2,1:T(8,128)S(1)}) fusion(f32[384,4,64]{0,2,1:T(8,128)S(1)} %fusion.68, f32[384,4]{0,1:T(4,128)S(1)} %bitcast.223, bf16[3072,4,128]{0,2,1:T(8,128)(2,1)} %all-gather.10.cloned.1.call-done, f32[4,384,3072]{2,1,0:T(8,128)} %get-tuple-element.257, f32[4,384]{1,0:T(4,128)S(1)} %get-tuple-element.264, ...), kind=kOutput, calls=%fused_computation.97 | convolution fusion | flops 628062720 | bytes 22431760 | tf_op jit(solution)/shard_map/hqk,khd->hqd/dot_general | solution.py:164
  262.1 0.6 fusion.133
  263.1 1.8 add_convert_fusion
  264.9 38.5 %reduce-scatter.2.cloned.1.call-done = bf16[384,512]{1,0:T(8,128)(2,1)} async-done(((bf16[384,2048]{1,0:T(8,128)(2,1)}), bf16[384,512]{1,0:T(8,128)(2,1)}) %reduce-scatter.2.cloned.1.call-update) | async-done | bytes 393232 | tf_op jit(solution)/shard_map/reduce_scatter | solution.py:273
  (136 shorter events, 9.0 us)
Async XLA Ops:
  6.5 255.5 %copy-start = (bf16[256,2048]{1,0:T(8,128)(2,1)S(1)}, bf16[256,2048]{1,0:T(8,128)(2,1)}, u32[]{:S(2)}) copy-start(bf16[256,2048]{1,0:T(8,128)(2,1)} %param.34) | copy-start | bytes 3145732
  6.5 26.6 %copy-start.19 = (f32[2048]{0:T(1024)S(1)}, f32[2048]{0:T(1024)}, u32[]{:S(2)}) copy-start(f32[2048]{0:T(1024)} %param.21) | copy-start | bytes 24580
  6.5 26.6 %copy-start.24 = (f32[384,4]{0,1:T(4,128)S(1)}, f32[384,4]{0,1:T(4,128)}, u32[]{:S(2)}) copy-start(f32[384,4]{0,1:T(4,128)} %param.31) | copy-start | bytes 18436
  6.5 26.6 %copy-start.25 = (f32[4]{0:T(128)S(1)}, f32[4]{0:T(128)}, u32[]{:S(2)}) copy-start(f32[4]{0:T(128)} %param.30) | copy-start | bytes 52
  6.5 26.6 %copy-start.16 = (bf16[2048,4]{0,1:T(4,128)(2,1)S(1)}, bf16[2048,4]{0,1:T(4,128)(2,1)}, u32[]{:S(2)}) copy-start(bf16[2048,4]{0,1:T(4,128)(2,1)} %param.29) | copy-start | bytes 49156
  6.5 30.5 %copy-start.17 = (bf16[2048,4]{0,1:T(4,128)(2,1)S(1)}, bf16[2048,4]{0,1:T(4,128)(2,1)}, u32[]{:S(2)}) copy-start(bf16[2048,4]{0,1:T(4,128)(2,1)} %param.28) | copy-start | bytes 49156
  6.6 24.8 %all-gather.8.cloned.1.call-start = ((), (), s32[]{:S(2)}) async-start(), calls=%async_computation.1 | async-start | bytes 1966080 | tf_op jit(solution)/shard_map/all_gather | solution.py:203
  7.3 191.0 %all-gather.10.cloned.1.call-start = ((), (), s32[]{:S(2)}) async-start(), calls=%async_computation.2 | async-start | bytes 3538944 | tf_op jit(solution)/shard_map/all_gather | solution.py:233
  10.2 198.3 %copy-start.2 = (pred[384,3072]{1,0:T(8,128)(4,1)}, pred[384,3072]{1,0:T(8,128)(4,1)S(1)}, u32[]{:S(2)}) copy-start(pred[384,3072]{1,0:T(8,128)(4,1)S(1)} %iota_compare_fusion) | copy-start | bytes 3538948
  33.2 84.0 %copy-start.10 = (f32[384]{0:T(512)}, f32[384]{0:T(512)S(1)}, u32[]{:S(2)}) copy-start(f32[384]{0:T(512)S(1)} %add_rsqrt_fusion.1) | copy-start | bytes 4612
  82.5 38.5 %copy-start.3 = (bf16[6,64,4,64]{3,2,1,0:T(4,128)(2,1)}, bf16[6,64,4,64]{3,2,1,0:T(4,128)(2,1)S(1)}, u32[]{:S(2)}) copy-start(bf16[6,64,4,64]{3,2,1,0:T(4,128)(2,1)S(1)} %reshape.198) | copy-start | bytes 589828
  82.5 32.1 %copy-start.20 = (f32[2048]{0:T(1024)S(1)}, f32[2048]{0:T(1024)}, u32[]{:S(2)}) copy-start(f32[2048]{0:T(1024)} %param.21) | copy-start | bytes 24580
  86.7 30.5 %copy-start.5 = (bf16[384,2048]{1,0:T(8,128)(2,1)S(1)}, bf16[384,2048]{1,0:T(8,128)(2,1)}, u32[]{:S(2)}) copy-start(bf16[384,2048]{1,0:T(8,128)(2,1)} %all-gather.8.cloned.1.call-done) | copy-start | bytes 4718596
  86.7 30.5 %copy-start.14 = (bf16[2048,256]{1,0:T(8,128)(2,1)S(1)}, bf16[2048,256]{1,0:T(8,128)(2,1)}, u32[]{:S(2)}) copy-start(bf16[2048,256]{1,0:T(8,128)(2,1)} %param.24) | copy-start | bytes 3145732
  86.7 30.5 %copy-start.21 = (f32[2048]{0:T(1024)S(1)}, f32[2048]{0:T(1024)}, u32[]{:S(2)}) copy-start(f32[2048]{0:T(1024)} %param.21) | copy-start | bytes 24580
  118.0 0.7 copy-start.8
  118.8 184.6 %reduce-scatter.2.cloned.1.call-start = ((), (), s32[]{:S(2)}) async-start(), calls=%async_computation.3 | async-start | bytes 1966080 | tf_op jit(solution)/shard_map/reduce_scatter | solution.py:273
  120.2 4.5 %copy-start.7 = (f32[4,64,64]{2,1,0:T(8,128)S(1)}, f32[4,64,64]{2,1,0:T(8,128)}, u32[]{:S(2)}) copy-start(f32[4,64,64]{2,1,0:T(8,128)} %fusion.84) | copy-start | bytes 196612
  161.6 18.9 %copy-start.11 = (f32[384]{0:T(512)S(1)}, f32[384]{0:T(512)}, u32[]{:S(2)}) copy-start(f32[384]{0:T(512)} %copy-done.10) | copy-start | bytes 4612
  161.6 18.9 %copy-start.22 = (f32[2048]{0:T(1024)S(1)}, f32[2048]{0:T(1024)}, u32[]{:S(2)}) copy-start(f32[2048]{0:T(1024)} %param.21) | copy-start | bytes 24580
  180.5 9.6 %copy-start.18 = (f32[6,4,64]{2,1,0:T(4,128)S(1)}, f32[6,4,64]{2,1,0:T(4,128)}, u32[]{:S(2)}) copy-start(f32[6,4,64]{2,1,0:T(4,128)} %get-tuple-element.126) | copy-start | bytes 18436
  183.6 9.7 %copy-start.4 = (bf16[6,64,4,64]{3,2,1,0:T(4,128)(2,1)S(1)}, bf16[6,64,4,64]{3,2,1,0:T(4,128)(2,1)}, u32[]{:S(2)}) copy-start(bf16[6,64,4,64]{3,2,1,0:T(4,128)(2,1)} %copy-done.3) | copy-start | bytes 589828
  189.5 4.7 %copy-start.9 = (bf16[4,6,64,64]{2,3,1,0:T(8,128)(2,1)S(1)}, bf16[4,6,64,64]{2,3,1,0:T(8,128)(2,1)}, u32[]{:S(2)}) copy-start(bf16[4,6,64,64]{2,3,1,0:T(8,128)(2,1)} %copy.80) | copy-start | bytes 589828
  189.5 4.7 %copy-start.15 = (f32[6,4,64,64]{3,2,0,1:T(8,128)S(1)}, f32[6,4,64,64]{3,2,0,1:T(8,128)}, u32[]{:S(2)}) copy-start(f32[6,4,64,64]{3,2,0,1:T(8,128)} %get-tuple-element.125) | copy-start | bytes 1179652
  193.3 2.3 copy-start.12
  193.3 2.3 copy-start.23
  226.1 17.9 %copy-start.1 = (f32[4,384,3072]{2,1,0:T(8,128)S(1)}, f32[4,384,3072]{2,1,0:T(8,128)}, u32[]{:S(2)}) copy-start(f32[4,384,3072]{2,1,0:T(8,128)} %fusion.75) | copy-start | bytes 56623108
  244.0 8.0 %copy-start.26 = (f32[4]{0:T(128)S(1)}, f32[4]{0:T(128)}, u32[]{:S(2)}) copy-start(f32[4]{0:T(128)} %param.32) | copy-start | bytes 52
  252.0 9.9 %copy-start.13 = (f32[64]{0:T(128)S(1)}, f32[64]{0:T(128)}, u32[]{:S(2)}) copy-start(f32[64]{0:T(128)} %param.33) | copy-start | bytes 772
  261.9 1.2 copy-start.6
Sparse Core Ops, SparseCore 0:
  8.9 22.3 all-gather.7
  118.9 66.6 all-gather.9
  265.0 38.3 reduce-scatter.1
where the time goes:
time: 311 us; the launch traced here: 310 us
  blocking collectives  101 us (32%)
  matrix products  75.5 us (24%)
  waiting for transfers between devices  60.4 us (19%)
  other arithmetic  36.2 us (12%)
  local copies, waits for them, and re-layouts  22.1 us (7%)
  between operations  14.4 us (5%)
    all_gather x3, blocking collectives, carried_in(): gathered = jax.tree.map(lambda a: lax.all_gather(a, axis), part)  79.7 us
    reduce_scatter x1, waiting for transfers between devices, per_device(): lax.psum_scatter(partial_term.astype(jnp.bfloat16), 'tp', scatter_dimensi...  38.5 us
    dot_general x2, matrix products, attend(): jnp.einsum('qhd,khd->hqk', query_side, key_side, preferred_element_type=j...  27.8 us
    unnamed x1, blocking collectives  21.3 us
    all_gather x1, waiting for transfers between devices, per_device(): lax.all_gather(inputs, 'tp', axis=1, tiled=True).astype(jnp.float32)  21.1 us
    dot_general x2, matrix products, attend(): jnp.einsum('hqk,khd->hqd', weights.astype(jnp.bfloat16), value_part, pref...  17.9 us
    dot_general x8, matrix products, per_device(): jnp.dot(scaled, weight, preferred_element_type=jnp.float32)  17.7 us
    reduce_sum x1, other arithmetic, attend(): totals = jnp.sum(weights, axis=2)  17.6 us
  transfers between devices with their start and end apart: 3, of which 2 were waited for; matrix products, arithmetic and copies ran while one was open for 14% of the time, Pallas kernels for 0%

commit v1 on v0

--- a/solution.py
+++ b/solution.py
@@ -9,6 +9,28 @@
 EPSILON = 1e-06
 ROTARY_BASE = 10000.0
 NEGATIVE = -1e30
+
+
+def joined_along(pieces, dim):
+    pieces = jnp.moveaxis(pieces, 0, dim)
+    shape = pieces.shape
+    return pieces.reshape(*shape[:dim], shape[dim] * shape[dim + 1], *shape[dim + 2 :])
+
+
+def gather_around(x, axis, dim):
+    size = lax.axis_size(axis)
+    pairs = [(i, (i + 1) % size) for i in range(size)]
+    back = [(b, a) for a, b in pairs]
+    lower, upper = ([], [])
+    for step in range(size - 1):
+        if step % 2 == 0:
+            lower.append(lax.ppermute(lower[-1] if lower else x, axis, pairs))
+        else:
+            upper.append(lax.ppermute(upper[-1] if upper else x, axis, back))
+    blocks = jnp.stack([*lower[::-1], x, *upper])
+    shift = lax.axis_index(axis) - len(lower)
+    blocks = blocks[(jnp.arange(size) - shift) % size]
+    return joined_along(blocks, dim)
 
 
 def carried_in(part, axis, combine, identity):
@@ -200,7 +222,7 @@
         input_gate_weight,
         forget_gate_weight,
     )
-    floats = lax.all_gather(inputs, "tp", axis=1, tiled=True).astype(jnp.float32)
+    floats = gather_around(inputs, "tp", 1).astype(jnp.float32)
     scaled = (floats * norm_gain[None, :]).astype(jnp.bfloat16)
     running_sums = tuple(
         (jnp.dot(scaled, weight, preferred_element_type=jnp.float32) for weight in weights)

time: 311 us -> 369 us (1.19)
  other arithmetic: 36.2 us -> 62.3 us
  local copies, waits for them, and re-layouts: 22.1 us -> 44 us
  starting transfers between devices: 0.12 us -> 5.28 us
  matrix products: 75.5 us -> 70.9 us
  blocking collectives: 101 us -> 105 us
  waiting for transfers between devices: 60.4 us -> 64.1 us
    all_gather x1 -> x0, waiting for transfers between devices: 21.1 us -> none  [per_device(): lax.all_gather(inputs, 'tp', axis=1, tiled=True).astype(jnp.float32)]
    reduce_scatter x1, waiting for transfers between devices: 38.5 us -> 56.7 us  [per_device(): lax.psum_scatter(partial_term.astype(jnp.bfloat16), 'tp', scatter_dimensi...]
    dynamic_update_slice x18, local copies, waits for them, and re-layouts: 7.69 us -> 19.4 us  [memory_blocks(): lax.scan(scan_step, entering, entries)]
    add x6, other arithmetic: 0.47 us -> 8.01 us  [advance_state(): former[:, None] * normal + latter[:, None] * block_normal]
    ppermute x0 -> x3, waiting for transfers between devices: none -> 7.37 us  [the longest x2 7.36 us: gather_around(): lower.append(lax.ppermute(lower[-1] if lower else x, axis, pairs))]
    dot_general x8, matrix products: 17.7 us -> 12.3 us  [per_device(): jnp.dot(scaled, weight, preferred_element_type=jnp.float32)]
    ppermute x0 -> x3, starting transfers between devices: none -> 5.06 us  [the longest x2 3.12 us: gather_around(): lower.append(lax.ppermute(lower[-1] if lower else x, axis, pairs))]
    convert_element_type x0 -> x2, other arithmetic: none -> 4.35 us  [the longest x1 2.26 us: per_device(): scaled = (floats * norm_gain[None, :]).astype(jnp.bfloat16)]
  transfers between devices with their start and end apart: 3 -> 5, of which waited for: 2 -> 3; matrix products, arithmetic and copies ran while one was open for 14% -> 21% of each run, Pallas kernels for 0% -> 0%
where the time goes in v1:
time: 369 us; the launch traced here: 366 us
  blocking collectives  105 us (28%)
  matrix products  70.9 us (19%)
  waiting for transfers between devices  64.1 us (17%)
  other arithmetic  62.3 us (17%)
  local copies, waits for them, and re-layouts  44 us (12%)
  between operations  14.7 us (4%)
  starting transfers between devices  5.28 us (1%)
    all_gather x3, blocking collectives, carried_in(): gathered = jax.tree.map(lambda a: lax.all_gather(a, axis), part)  81.4 us
    reduce_scatter x1, waiting for transfers between devices, per_device(): lax.psum_scatter(partial_term.astype(jnp.bfloat16), 'tp', scatter_dimensi...  56.7 us
    dot_general x2, matrix products, attend(): jnp.einsum('qhd,khd->hqk', query_side, key_side, preferred_element_type=j...  27.9 us
    unnamed x1, blocking collectives  23.2 us
    dynamic_update_slice x18, local copies, waits for them, and re-layouts, memory_blocks(): lax.scan(scan_step, entering, entries)  19.4 us
    dot_general x2, matrix products, attend(): jnp.einsum('hqk,khd->hqd', weights.astype(jnp.bfloat16), value_part, pref...  17.9 us
    reduce_sum x1, other arithmetic, attend(): totals = jnp.sum(weights, axis=2)  17.6 us
    dot_general x8, matrix products, per_device(): jnp.dot(scaled, weight, preferred_element_type=jnp.float32)  12.3 us
  transfers between devices with their start and end apart: 5, of which 3 were waited for; matrix products, arithmetic and copies ran while one was open for 21% of the time, Pallas kernels for 0%

profile of v1, /device:TPU:0, one launch (start us, length us, event | category | flops | bytes accessed | tf_op | source)
XLA Modules:
  0.0 366.0 jit_solution(16328556847652764098)
XLA Ops:
  7.0 1.9 collective-permute-start.2
  9.0 1.7 iota_compare_fusion
  10.7 5.5 %collective-permute-done = bf16[384,512]{1,0:T(8,128)(2,1)S(1)} collective-permute-done((bf16[384,512]{1,0:T(8,128)(2,1)}, bf16[384,512]{1,0:T(8,128)(2,1)S(1)}, u32[]{:S(2)}, u32[]{:S(2)}) %collective-permute-start) | collective-permute-done | bytes 393248 | tf_op jit(solution)/shard_map/ppermute | solution.py:27
  16.3 2.6 collective-permute-start.1
  18.9 1.2 dynamic-slice
  21.6 1.9 collective-permute-done.1
  23.5 2.4 pad_maximum_fusion
  25.8 2.1 gather_fusion
  28.3 2.1 convert_bitcast_fusion
  30.4 3.6 copy.74
  34.0 2.3 fusion.26
  36.7 1.2 reduce-window.6
  39.4 23.2 %all-reduce = f32[32]{0:T(128)S(1)} all-reduce(f32[32]{0:T(128)S(1)} %dynamic-update-slice), channel_id=2, replica_groups=mesh['sp'=8,'tp'=4] {'sp'}, use_global_device_ids=true, to_apply=%add | all-reduce | flops 32 | bytes 256
  63.3 17.0 %all-gather.3 = f32[8,1,4]{2,1,0:T(1,128)} all-gather(f32[1,1,4]{2,1,0:T(1,128)S(1)} %bitcast.246), channel_id=1, replica_groups=mesh['sp'=8,'tp'=4] {'sp'}, dimensions={0}, use_global_device_ids=true | all-gather | bytes 144 | tf_op jit(solution)/shard_map/all_gather | solution.py:38
  82.9 2.0 fusion.46
  86.8 2.7 fusion.45
  89.6 1.4 fusion.44
  93.9 26.9 %all-gather.4 = f32[8,4,64]{2,1,0:T(4,128)} all-gather(f32[1,4,64]{2,1,0:T(4,128)S(1)} %bitcast.245), channel_id=4, replica_groups=mesh['sp'=8,'tp'=4] {'sp'}, dimensions={0}, use_global_device_ids=true | all-gather | bytes 9216 | tf_op jit(solution)/shard_map/all_gather | solution.py:38
  123.9 1.3 mul.425
  125.2 2.1 fusion.81
  127.3 1.6 convert_multiply_fusion.1
  128.9 2.3 fusion.78
  131.2 37.5 %all-gather.1 = f32[32,64,64]{2,1,0:T(8,128)} all-gather(f32[4,64,64]{2,1,0:T(8,128)S(1)} %fusion.84), channel_id=3, replica_groups=mesh['sp'=8,'tp'=4] {'sp'}, dimensions={0}, use_global_device_ids=true | all-gather | bytes 589824 | tf_op jit(solution)/shard_map/all_gather | solution.py:38
  171.8 1.3 multiply_add_fusion.1
  174.1 44.7 %while.37 = (s32[]{:T(128)}, f32[4,64,64]{2,1,0:T(8,128)S(1)}, f32[4,64]{1,0:T(4,128)}, f32[4]{0:T(128)}, f32[6,4,64,64]{3,2,0,1:T(8,128)}, /*index=5*/f32[6,4,6...) while((s32[]{:T(128)}, f32[4,64,64]{2,1,0:T(8,128)S(1)}, ...), condition=%wide.region_14.15_spmd, body=%wide.region_13.14_spmd.sunk | while | flops 49938 | bytes 400769 | solution.py:109
  174.1 1.3 dynamic_update_slice.19
  175.4 1.2 subtract_exponential_fusion.13
  177.3 1.3 bitcast_dynamic-update-slice_fusion.5
  178.5 1.3 fusion.160
  180.6 1.0 fusion.159
  181.6 1.3 dynamic_update_slice.19
  182.9 1.2 subtract_exponential_fusion.13
  184.7 1.3 bitcast_dynamic-update-slice_fusion.5
  186.0 1.3 fusion.160
  189.0 1.3 dynamic_update_slice.19
  190.3 1.2 subtract_exponential_fusion.13
  192.2 1.3 bitcast_dynamic-update-slice_fusion.5
  193.4 1.3 fusion.160
  196.5 1.3 dynamic_update_slice.19
  197.8 1.2 subtract_exponential_fusion.13
  199.6 1.3 bitcast_dynamic-update-slice_fusion.5
  200.9 1.3 fusion.160
  203.9 1.3 dynamic_update_slice.19
  205.2 1.2 subtract_exponential_fusion.13
  207.1 1.3 bitcast_dynamic-update-slice_fusion.5
  208.4 1.3 fusion.160
  211.4 1.3 dynamic_update_slice.19
  212.7 1.2 subtract_exponential_fusion.13
  214.5 1.3 bitcast_dynamic-update-slice_fusion.5
  215.8 1.3 fusion.160
  218.9 2.7 fusion.50
  221.5 1.7 copy.87
  223.3 1.9 reshape.251
  225.2 2.0 copy.103
  227.9 1.4 fusion.101
  229.4 1.7 fusion.124
  233.6 2.0 fusion.43
  235.7 10.3 %fusion.75 = f32[4,384,3072]{2,1,0:T(8,128)} fusion(bf16[3072,4,128]{0,2,1:T(8,128)(2,1)} %all-gather.7.cloned.1.call-done, bf16[384,4,16]{0,2,1:T(8,128)(2,1)S(1)} %get-tuple-element.274, bf16[384,4,16]{0,2,1:T(8,128)(2,1)S(1)} %get-tuple-element.275), kind=kOutput, calls=%fused_computation.85 | convolution fusion | flops 302186496 | bytes 19759104 | tf_op jit(solution)/shard_map/qhd,khd->hqk/dot_general | solution.py:179
  246.1 17.6 %fusion.14 = (f32[4,384]{1,0:T(4,128)S(1)}, f32[4,384]{1,0:T(4,128)S(1)}, f32[4,384,3072]{2,1,0:T(8,128)}) fusion(pred[384,3072]{1,0:T(8,128)(4,1)S(1)} %copy-done.2, f32[4,384,3072]{2,1,0:T(8,128)} %fusion.75, bf16[3072,4,128]{0,2,1:T(8,128)(2,1)} %all-gather.7.cloned.1.call-done, bf16[384,4,16]{0,2,1:T(8,128)(2,1)S(1)} %get-tuple-element.267, ...), kind=kOutput, calls=%fused_computation.33 | convolution fusion | flops 330494976 | bytes 39825408 | tf_op jit(solution)/shard_map/qhd,khd->hqk/dot_general | solution.py:179
  263.7 17.6 %fusion.17 = (f32[4,384]{1,0:T(4,128)S(1)}, f32[4,384]{1,0:T(4,128)S(1)}) fusion(f32[4,384,3072]{2,1,0:T(8,128)} %get-tuple-element.278, f32[4,384]{1,0:T(4,128)S(1)} %get-tuple-element.285, pred[384,3072]{1,0:T(8,128)(4,1)} %iota_compare_fusion, f32[4,384]{1,0:T(4,128)S(1)} %get-tuple-element.286, f32[4,384,3072]{2,1,0:T(8,128)} %fusion.75), kind=kLoop, calls=%fused_computation.36 | loop fusion | flops 47182848 | bytes 38952960 | tf_op jit(solution)/shard_map/reduce_sum | solution.py:185
  281.5 8.0 %fusion.68 = f32[384,4,64]{0,2,1:T(8,128)S(1)} fusion(bf16[3072,4,128]{0,2,1:T(8,128)(2,1)} %all-gather.7.cloned.1.call-done, f32[4,384,3072]{2,1,0:T(8,128)S(1)} %copy-done.1, f32[4,384]{1,0:T(4,128)S(1)} %get-tuple-element.286, pred[384,3072]{1,0:T(8,128)(4,1)} %iota_compare_fusion, f32[384,4]{0,1:T(4,128)S(1)} %bitcast.249), kind=kOutput, calls=%fused_computation.82 | convolution fusion | flops 627671040 | bytes 22032384 | tf_op jit(solution)/shard_map/hqk,khd->hqd/dot_general | solution.py:186
  289.5 9.9 %multiply_reduce_fusion = (f32[384,4]{0,1:T(4,128)S(1)}, f32[384,4,64]{0,2,1:T(8,128)S(1)}) fusion(f32[384,4,64]{0,2,1:T(8,128)S(1)} %fusion.68, f32[384,4]{0,1:T(4,128)S(1)} %bitcast.248, bf16[3072,4,128]{0,2,1:T(8,128)(2,1)} %all-gather.7.cloned.1.call-done, f32[4,384,3072]{2,1,0:T(8,128)} %get-tuple-element.278, f32[4,384]{1,0:T(4,128)S(1)} %get-tuple-element.285, ...), kind=kOutput, calls=%fused_computation.100 | convolution fusion | flops 628062720 | bytes 22431760 | tf_op jit(solution)/shard_map/hqk,khd->hqd/dot_general | solution.py:186
  300.7 1.8 add_convert_fusion
  302.5 56.7 %reduce-scatter.2.cloned.1.call-done = bf16[384,512]{1,0:T(8,128)(2,1)} async-done(((bf16[384,2048]{1,0:T(8,128)(2,1)}), bf16[384,512]{1,0:T(8,128)(2,1)}) %reduce-scatter.2.cloned.1.call-update) | async-done | bytes 393232 | tf_op jit(solution)/shard_map/reduce_scatter | solution.py:295
  (154 shorter events, 36.6 us)
Async XLA Ops:
  6.5 293.1 %copy-start = (bf16[256,2048]{1,0:T(8,128)(2,1)S(1)}, bf16[256,2048]{1,0:T(8,128)(2,1)}, u32[]{:S(2)}) copy-start(bf16[256,2048]{1,0:T(8,128)(2,1)} %param.34) | copy-start | bytes 3145732
  6.5 229.2 %all-gather.7.cloned.1.call-start = ((), (), s32[]{:S(2)}) async-start(), calls=%async_computation.1 | async-start | bytes 3538944 | tf_op jit(solution)/shard_map/all_gather | solution.py:255
  6.5 9.7 %collective-permute-start = (bf16[384,512]{1,0:T(8,128)(2,1)}, bf16[384,512]{1,0:T(8,128)(2,1)S(1)}, u32[]{:S(2)}, u32[]{:S(2)}) collective-permute-start(bf16[384,512]{1,0:T(8,128)(2,1)} %param.20), channel_id=1, source_target_pairs={{0,1},{1,2},{2,3},{3,0},{4,5},{5,6},{6,7},{7,4},{8,9},{9,10},{10,1... | collective-permute-start | bytes 1179656 | tf_op jit(solution)/shard_map/ppermute | solution.py:27
  7.0 14.6 %collective-permute-start.2 = (bf16[384,512]{1,0:T(8,128)(2,1)}, bf16[384,512]{1,0:T(8,128)(2,1)S(1)}, u32[]{:S(2)}, u32[]{:S(2)}) collective-permute-start(bf16[384,512]{1,0:T(8,128)(2,1)} %param.20), channel_id=1, source_target_pairs={{1,0},{2,1},{3,2},{0,3},{5,4},{6,5},{7,6},{4,7},{9,8},{10,9},{11,1... | collective-permute-start | bytes 1179656 | tf_op jit(solution)/shard_map/ppermute | solution.py:29
  16.3 7.2 %collective-permute-start.1 = (bf16[384,512]{1,0:T(8,128)(2,1)S(1)}, bf16[384,512]{1,0:T(8,128)(2,1)S(1)}, u32[]{:S(2)}, u32[]{:S(2)}) collective-permute-start(bf16[384,512]{1,0:T(8,128)(2,1)S(1)} %collective-permute-done), channel_id=1, source_target_pairs={{0,1},{1,2},{2,3},{3,0},{4,5},{5,6},{6,7},{7,4},{8,9},{9,10},{10,1... | collective-permute-start | bytes 1179656 | tf_op jit(solution)/shard_map/ppermute | solution.py:27
  21.6 100.3 %copy-start.6 = (f32[384,16]{0,1:T(8,128)}, f32[384,16]{0,1:T(8,128)S(1)}, u32[]{:S(2)}) copy-start(f32[384,16]{0,1:T(8,128)S(1)} %get-tuple-element.276) | copy-start | bytes 73732
  21.6 100.3 %copy-start.8 = (f32[384,16]{0,1:T(8,128)}, f32[384,16]{0,1:T(8,128)S(1)}, u32[]{:S(2)}) copy-start(f32[384,16]{0,1:T(8,128)S(1)} %get-tuple-element.277) | copy-start | bytes 73732
  30.4 60.7 %copy-start.17 = (f32[384]{0:T(512)}, f32[384]{0:T(512)S(1)}, u32[]{:S(2)}) copy-start(f32[384]{0:T(512)S(1)} %add_rsqrt_fusion.1) | copy-start | bytes 4612
  30.4 3.6 copy-start.22
  34.0 2.3 copy-start.19
  34.0 2.3 copy-start.23
  34.0 2.3 copy-start.24
  34.0 4.5 %copy-start.20 = (bf16[2048,4]{0,1:T(4,128)(2,1)S(1)}, bf16[2048,4]{0,1:T(4,128)(2,1)}, u32[]{:S(2)}) copy-start(bf16[2048,4]{0,1:T(4,128)(2,1)} %param.28) | copy-start | bytes 49156
  39.0 50.5 %copy-start.12 = (f32[6,64,4]{1,0,2:T(8,128)}, f32[6,64,4]{1,0,2:T(8,128)S(1)}, u32[]{:S(2)}) copy-start(f32[6,64,4]{1,0,2:T(8,128)S(1)} %reshape.249) | copy-start | bytes 18436
  81.6 8.0 %copy-start.15 = (f32[4,6,64]{2,1,0:T(8,128)}, f32[4,6,64]{2,1,0:T(8,128)S(1)}, u32[]{:S(2)}) copy-start(f32[4,6,64]{2,1,0:T(8,128)S(1)} %subtract_exponential_fusion.4) | copy-start | bytes 18436
  86.8 2.7 copy-start.26
  89.6 1.5 copy-start.27
  122.9 0.7 copy-start.10
  123.7 235.6 %reduce-scatter.2.cloned.1.call-start = ((), (), s32[]{:S(2)}) async-start(), calls=%async_computation.2 | async-start | bytes 1966080 | tf_op jit(solution)/shard_map/reduce_scatter | solution.py:295
  170.4 2.7 copy-start.3
  171.1 3.0 copy-start.14
  218.8 8.3 %copy-start.21 = (f32[6,4]{1,0:T(8,128)S(1)}, f32[6,4]{1,0:T(8,128)}, u32[]{:S(2)}) copy-start(f32[6,4]{1,0:T(8,128)} %get-tuple-element.124) | copy-start | bytes 292
  218.8 8.5 %copy-start.13 = (f32[6,64,4]{1,0,2:T(8,128)S(1)}, f32[6,64,4]{1,0,2:T(8,128)}, u32[]{:S(2)}) copy-start(f32[6,64,4]{1,0,2:T(8,128)} %copy-done.12) | copy-start | bytes 18436
  218.8 8.5 %copy-start.16 = (pred[64,64]{0,1:T(8,128)(4,1)S(1)}, pred[64,64]{0,1:T(8,128)(4,1)}, u32[]{:S(2)}) copy-start(pred[64,64]{0,1:T(8,128)(4,1)} %iota_compare_fusion.1) | copy-start | bytes 12292
  218.8 9.1 %copy-start.29 = (f32[6,4,64]{2,1,0:T(4,128)S(1)}, f32[6,4,64]{2,1,0:T(4,128)}, u32[]{:S(2)}) copy-start(f32[6,4,64]{2,1,0:T(4,128)} %get-tuple-element.126) | copy-start | bytes 18436
  227.3 3.9 %copy-start.4 = (bf16[6,64,4,64]{3,2,1,0:T(4,128)(2,1)S(1)}, bf16[6,64,4,64]{3,2,1,0:T(4,128)(2,1)}, u32[]{:S(2)}) copy-start(bf16[6,64,4,64]{3,2,1,0:T(4,128)(2,1)} %reshape.250) | copy-start | bytes 589828
  227.3 4.7 %copy-start.11 = (bf16[4,6,64,64]{2,3,1,0:T(8,128)(2,1)S(1)}, bf16[4,6,64,64]{2,3,1,0:T(8,128)(2,1)}, u32[]{:S(2)}) copy-start(bf16[4,6,64,64]{2,3,1,0:T(8,128)(2,1)} %copy.103) | copy-start | bytes 589828
  227.3 4.7 %copy-start.28 = (f32[6,4,64,64]{3,2,0,1:T(8,128)S(1)}, f32[6,4,64,64]{3,2,0,1:T(8,128)}, u32[]{:S(2)}) copy-start(f32[6,4,64,64]{3,2,0,1:T(8,128)} %get-tuple-element.125) | copy-start | bytes 1179652
  231.2 2.4 copy-start.18
  233.0 2.7 copy-start.7
  233.0 2.7 copy-start.9
  235.7 10.4 %copy-start.2 = (pred[384,3072]{1,0:T(8,128)(4,1)S(1)}, pred[384,3072]{1,0:T(8,128)(4,1)}, u32[]{:S(2)}) copy-start(pred[384,3072]{1,0:T(8,128)(4,1)} %iota_compare_fusion) | copy-start | bytes 3538948
  263.7 17.9 %copy-start.1 = (f32[4,384,3072]{2,1,0:T(8,128)S(1)}, f32[4,384,3072]{2,1,0:T(8,128)}, u32[]{:S(2)}) copy-start(f32[4,384,3072]{2,1,0:T(8,128)} %fusion.75) | copy-start | bytes 56623108
  281.5 8.0 %copy-start.30 = (f32[4]{0:T(128)S(1)}, f32[4]{0:T(128)}, u32[]{:S(2)}) copy-start(f32[4]{0:T(128)} %param.32) | copy-start | bytes 52
  289.5 10.0 %copy-start.25 = (f32[64]{0:T(128)S(1)}, f32[64]{0:T(128)}, u32[]{:S(2)}) copy-start(f32[64]{0:T(128)} %param.33) | copy-start | bytes 772
  299.5 1.2 copy-start.5
Sparse Core Ops, SparseCore 0:
  123.8 68.7 all-gather.6
  302.6 56.5 reduce-scatter.1
